TPU v7x, 128 devices: a whole 4x4x4 slice. The times are simulated.
128 devices in a mesh: sp: 32 (over z, y, core), tp: 4 (over x).
Axes of the slice: x: 4, y: 4, z: 4, core: 2. Of those that a mesh axis runs over, the one named last changes fastest.
Arguments:
- conv_input: bfloat16 [16384, 1024], P('sp', 'tp'), may hold values from -6 to 6
- gate_inner: bfloat16 [16384, 1024], P('sp', 'tp'), may hold values from -6 to 6
- gate_outer: bfloat16 [16384, 1024], P('sp', 'tp'), may hold values from -6 to 6
- conv_taps: bfloat16 [3, 1024], P(None, 'tp'), may hold values from -3.5 to 3.5
- doc_ids: int32 [16384], P('sp'), may hold values from 0 to 15, never falling along the last dimension, each value on 1 to 2048 neighbouring positions
- residual_in: bfloat16 [16384, 2048], P(('sp', 'tp')), may hold values from -6 to 6
- out_proj: bfloat16 [1024, 2048], replicated, may hold values from -0.1875 to 0.1875
- norm_gain: float32 [2048], replicated, may hold values from 0.1 to 1.9
- expert_ids: int32 [16384, 2], P(('sp', 'tp')), may hold values from 0 to 127, all different within a row; in each aligned block of 128 rows (0 to 127, 128 to 255, ...) at most 4 rows name the same one
- expert_weights: float32 [16384, 2], P(('sp', 'tp')), may hold values from 0.2 to 1
- gate_proj: bfloat16 [128, 2048, 1024], P(('sp', 'tp')), may hold values from -0.125 to 0.125
- up_proj: bfloat16 [128, 2048, 1024], P(('sp', 'tp')), may hold values from -0.125 to 0.125
- down_proj: bfloat16 [128, 1024, 2048], P(('sp', 'tp')), may hold values from -0.1875 to 0.1875
Outputs:
- layer_out: bfloat16 [16384, 2048], P(('sp', 'tp'))
Inputs may be any that keep to these rules, and one draw needn't show every extreme that they name: `doc_ids`: never falls along positions; each document has at most 2048 positions. `expert_ids`: each row names 2 different experts; within the rows of one device, aligned blocks of 128 rows, no expert is named more than 4 times, a bound that some block reaches.
All inputs are finite; a program needn't handle non-finite values.
Results may differ from a plain program's by a relative error of at most 0.009.
Values may be sent and summed in bfloat16 or wider, within the bound.
No kernel may reach another device: no remote copies, remote signals or barrier semaphores. Data moves between devices by JAX's collectives and lax.ppermute only.
A program may use at most 64 MiB of HBM per device.

v0:
```python
import jax
import jax.numpy as jnp
from jax import lax
from jax.sharding import PartitionSpec as P


def from_behind(block, axis, distance):
    devices = range(lax.axis_size(axis))
    route = [(i - distance, i) for i in devices if i - distance in devices]
    return lax.ppermute(block, axis, route)


def expert_rows(arrived, gate_weight, up_weight, down_weight):
    gate_value = jnp.dot(arrived, gate_weight, preferred_element_type=jnp.float32)
    up_value = jnp.dot(arrived, up_weight, preferred_element_type=jnp.float32)
    hidden = (jax.nn.silu(gate_value) * up_value).astype(jnp.bfloat16)
    return jnp.dot(hidden, down_weight, preferred_element_type=jnp.float32).astype(jnp.bfloat16)


def on_device(
    conv_input,
    gate_inner,
    gate_outer,
    conv_taps,
    doc_ids,
    residual_in,
    out_proj,
    norm_gain,
    expert_ids,
    expert_weights,
    gate_proj,
    up_proj,
    down_proj,
):
    inner_prod = conv_input.astype(jnp.float32) * gate_inner.astype(jnp.float32)
    earlier, earlier_docs = from_behind((inner_prod[-2:], doc_ids[-2:]), "sp", 1)
    padded = jnp.concatenate([earlier, inner_prod], axis=0)
    padded_docs = jnp.concatenate([earlier_docs, doc_ids], axis=0)
    length = inner_prod.shape[0]
    tap_values = conv_taps.astype(jnp.float32)
    one_back = jnp.where(
        (padded_docs[1 : length + 1] == doc_ids)[:, None], padded[1 : length + 1], 0.0
    )
    two_back = jnp.where((padded_docs[:length] == doc_ids)[:, None], padded[:length], 0.0)
    mixed_rows = tap_values[2] * inner_prod + tap_values[1] * one_back + tap_values[0] * two_back
    conv_out = (gate_outer.astype(jnp.float32) * mixed_rows).astype(jnp.bfloat16)
    row_count = residual_in.shape[0]
    regrouped = lax.all_to_all(conv_out, "tp", split_axis=0, concat_axis=1, tiled=True)
    mix = jnp.dot(regrouped, out_proj, preferred_element_type=jnp.float32).astype(jnp.bfloat16)
    carried = residual_in.astype(jnp.float32) + mix.astype(jnp.float32)
    normed = (
        carried * lax.rsqrt(jnp.mean(carried * carried, axis=1, keepdims=True) + 1e-06) * norm_gain
    ).astype(jnp.bfloat16)
    model_width = normed.shape[1]
    choose = expert_ids.shape[1]
    sp_count = lax.axis_size("sp")
    tp_count = lax.axis_size("tp")
    experts_total = sp_count * tp_count
    capacity = 2 * row_count * choose // experts_total
    flat_ids = expert_ids.reshape(-1)
    onehot = (flat_ids[:, None] == jnp.arange(experts_total, dtype=jnp.int32)[None, :]).astype(
        jnp.int32
    )
    slot_rank = jnp.sum((jnp.cumsum(onehot, axis=0) - 1) * onehot, axis=1)
    target = flat_ids * capacity + slot_rank
    sources = jnp.repeat(normed, choose, axis=0)
    outgoing = (
        jnp.zeros((experts_total * capacity, model_width), jnp.bfloat16).at[target].set(sources)
    )
    gate_weight = gate_proj[0]
    up_weight = up_proj[0]
    down_weight = down_proj[0]
    arrived = lax.all_to_all(
        outgoing.reshape(experts_total, capacity, model_width),
        ("sp", "tp"),
        split_axis=0,
        concat_axis=0,
        tiled=True,
    )
    item_count = arrived.shape[1]
    flat_rows = arrived.reshape(-1, model_width)
    result = expert_rows(flat_rows, gate_weight, up_weight, down_weight)
    result = result.reshape(experts_total, item_count, model_width)
    returned = lax.all_to_all(result, ("sp", "tp"), split_axis=0, concat_axis=0, tiled=True)
    picked = (
        returned.reshape(-1, model_width)[target]
        .reshape(row_count, choose, model_width)
        .astype(jnp.float32)
    )
    combined = carried + jnp.sum(expert_weights[:, :, None] * picked, axis=1)
    return combined.astype(jnp.bfloat16)


def solution(mesh):
    in_specs = (
        P("sp", "tp"),
        P("sp", "tp"),
        P("sp", "tp"),
        P(None, "tp"),
        P("sp"),
        P(("sp", "tp"), None),
        P(),
        P(),
        P(("sp", "tp"), None),
        P(("sp", "tp"), None),
        P(("sp", "tp"), None, None),
        P(("sp", "tp"), None, None),
        P(("sp", "tp"), None, None),
    )
    out_specs = P(("sp", "tp"), None)
    return jax.shard_map(
        on_device, mesh=mesh, in_specs=in_specs, out_specs=out_specs, check_vma=False
    )
```

profile of v0, /device:TPU:1, one launch (start us, length us, event | category | flops | bytes accessed | tf_op | source)
XLA Modules:
  0.0 143.9 jit_solution(9995977291659634800)
XLA Ops:
  0.0 1.2 convert_multiply_fusion
  1.2 4.6 %collective-permute-start.1 = (f32[2,256]{1,0:T(2,128)S(1)}, f32[2,256]{1,0:T(2,128)S(1)}, u32[]{:S(2)}, u32[]{:S(2)}) collective-permute-start(f32[2,256]{1,0:T(2,128)S(1)} %slice.48), channel_id=1, source_target_pairs={{0,4},{4,8},{8,12},{12,16},{16,20},{20,24},{24,28},{28,32},{32,36}... | collective-permute-start | bytes 6152 | tf_op jit(solution)/shard_map/ppermute | solution.py:10
  5.8 0.8 slice.35
  6.5 1.9 %collective-permute-start = (s32[2]{0:T(128)S(1)}, s32[2]{0:T(128)S(1)}, u32[]{:S(2)}, u32[]{:S(2)}) collective-permute-start(s32[2]{0:T(128)S(1)} %slice.35), channel_id=1, source_target_pairs={{0,4},{4,8},{8,12},{12,16},{16,20},{20,24},{24,28},{28,32},{32,36}... | collective-permute-start | bytes 32 | tf_op jit(solution)/shard_map/ppermute | solution.py:10
  8.4 0.8 copy.24
  9.4 0.1 eq.33
  9.5 0.7 broadcast_multiply_fusion
  10.2 0.8 fusion.31
  11.1 0.2 fusion.26
  11.7 0.2 fusion.27
  12.1 1.0 fusion.23
  13.1 4.0 %all-to-all-start = ((bf16[4,128,256]{2,1,0:T(8,128)(2,1)}), bf16[4,128,256]{2,1,0:T(8,128)(2,1)S(1)}, u32[]{:S(2)}, u32[]{:S(2)}) async-start(bf16[4,128,256]{2,1,0:T(8,128)(2,1)} %bitcast.3), calls=%async_computation | async-start | bytes 524288 | tf_op jit(solution)/shard_map/all_to_all | solution.py:48
  17.1 5.7 %all-to-all-done = bf16[4,128,256]{2,1,0:T(8,128)(2,1)S(1)} async-done(((bf16[4,128,256]{2,1,0:T(8,128)(2,1)}), bf16[4,128,256]{2,1,0:T(8,128)(2,1)S(1)}, u32[]{:S(2)}, u32[]{:S(2)}) %all-to-all-start) | async-done | bytes 262176 | tf_op jit(solution)/shard_map/all_to_all | solution.py:48
  22.8 0.2 copy.21
  23.0 3.0 %multiply_reduce_fusion.1 = (f32[128]{0:T(128)S(1)}, f32[128,2048]{1,0:T(8,128)S(1)}) fusion(bf16[128,1024]{0,1:T(8,128)(2,1)S(1)} %bitcast.35, bf16[1024,2048]{1,0:T(8,128)(2,1)} %param.19, bf16[128,2048]{1,0:T(8,128)(2,1)S(1)} %copy-done.1), kind=kOutput, calls=%fused_computation.16 | convolution fusion | flops 538443648 | bytes 6029824 | tf_op jit(solution)/shard_map/dot_general | solution.py:49
  26.0 0.2 multiply_convert_fusion.1
  26.2 0.6 broadcast_in_dim.36
  26.8 1.2 reshape.100
  28.1 3.5 %scatter_custom_fusion = bf16[512,2048]{1,0:T(8,128)(2,1)S(1)} fusion(s32[256]{0:T(256)S(1)} %bitcast.38, bf16[256,2048]{1,0:T(8,128)(2,1)} %reshape.100, bf16[]{:T(256)} %constant.6.clone.1), kind=kCustom, calls=%fused_computation.17 | custom fusion | bytes 2097664 | tf_op jit(solution)/shard_map/scatter | solution.py:68
  31.6 2.2 %reshape.83 = bf16[128,4,2048]{2,1,0:T(4,128)(2,1)} reshape(bf16[512,2048]{1,0:T(8,128)(2,1)S(1)} %scatter_custom_fusion) | data formatting | bytes 4194304 | tf_op jit(solution)/shard_map/reshape | solution.py:74
  33.8 40.5 %all_to_all.29 = bf16[128,4,2048]{2,1,0:T(4,128)(2,1)S(1)} all-to-all(bf16[128,4,2048]{2,1,0:T(4,128)(2,1)} %reshape.83), channel_id=1, replica_groups=mesh['sp'=32,'tp'=4] {'sp','tp'}, dimensions={0} | all-to-all | bytes 4194304 | tf_op jit(solution)/shard_map/all_to_all | solution.py:73
  74.3 2.0 %reshape.84 = bf16[512,2048]{1,0:T(8,128)(2,1)} reshape(bf16[128,4,2048]{2,1,0:T(4,128)(2,1)S(1)} %all_to_all.29) | data formatting | bytes 4194304 | tf_op jit(solution)/shard_map/reshape | solution.py:81
  76.4 6.6 %fusion.4 = f32[512,1024]{1,0:T(8,128)} fusion(bf16[512,2048]{1,0:T(8,128)(2,1)} %reshape.84, bf16[1,2048,1024]{2,1,0:T(8,128)(2,1)} %param.23), kind=kOutput, calls=%fused_computation.6 | convolution fusion | flops 2147483648 | bytes 8388608 | tf_op jit(solution)/shard_map/dot_general | solution.py:14
  83.0 9.9 %fusion.6 = bf16[512,2048]{1,0:T(8,128)(2,1)} fusion(bf16[1,1024,2048]{2,1,0:T(8,128)(2,1)} %param.25, f32[512,1024]{1,0:T(8,128)} %fusion.4, bf16[512,2048]{1,0:T(8,128)(2,1)S(1)} %copy-done, bf16[1,2048,1024]{2,1,0:T(8,128)(2,1)} %param.24), kind=kOutput, calls=%fused_computation.8 | convolution fusion | flops 4299161600 | bytes 14680064 | tf_op jit(solution)/shard_map/dot_general | solution.py:17
  92.9 4.1 %reshape.85 = bf16[128,4,2048]{2,1,0:T(4,128)(2,1)} reshape(bf16[512,2048]{1,0:T(8,128)(2,1)} %fusion.6) | data formatting | bytes 4194304 | tf_op jit(solution)/shard_map/reshape | solution.py:83
  97.0 5.0 %all-to-all-start.2 = ((bf16[128,4,2048]{2,1,0:T(4,128)(2,1)}), bf16[128,4,2048]{2,1,0:T(4,128)(2,1)}, u32[]{:S(2)}, u32[]{:S(2)}) async-start(bf16[128,4,2048]{2,1,0:T(4,128)(2,1)} %reshape.85), calls=%async_computation.2 | async-start | bytes 4194304 | tf_op jit(solution)/shard_map/all_to_all | solution.py:84
  102.1 30.4 %all-to-all-done.2 = bf16[128,4,2048]{2,1,0:T(4,128)(2,1)} async-done(((bf16[128,4,2048]{2,1,0:T(4,128)(2,1)}), bf16[128,4,2048]{2,1,0:T(4,128)(2,1)}, u32[]{:S(2)}, u32[]{:S(2)}) %all-to-all-start.2) | async-done | bytes 2097184 | tf_op jit(solution)/shard_map/all_to_all | solution.py:84
  132.6 2.5 %reshape.86 = bf16[512,2048]{1,0:T(8,128)(2,1)S(1)} reshape(bf16[128,4,2048]{2,1,0:T(4,128)(2,1)} %all-to-all-done.2) | data formatting | bytes 4194304 | tf_op jit(solution)/shard_map/reshape | solution.py:86
  135.1 2.3 %gather_fusion = bf16[256,2048]{1,0:T(8,128)(2,1)} fusion(bf16[512,2048]{1,0:T(8,128)(2,1)S(1)} %reshape.86, s32[1024]{0:T(1024)S(1)} %pad_clamp_fusion), kind=kCustom, calls=%fused_computation | custom fusion | bytes 2098176 | tf_op jit(solution)/shard_map/gather | solution.py:86
  137.4 2.4 %reshape.87 = f32[128,2,2048]{2,1,0:T(2,128)S(1)} reshape(bf16[256,2048]{1,0:T(8,128)(2,1)} %gather_fusion) | data formatting | bytes 3145728 | tf_op jit(solution)/shard_map/convert_element_type | solution.py:88
  139.8 3.2 %multiply_reduce_fusion = f32[128,2048]{1,0:T(8,128)S(1)} fusion(f32[128,2,2048]{2,1,0:T(2,128)S(1)} %reshape.87, f32[128,2]{1,0:T(8,128)S(1)} %copy.22), kind=kLoop, calls=%fused_computation.12 | loop fusion | flops 786432 | bytes 3146752 | tf_op jit(solution)/shard_map/reduce_sum | solution.py:90
  143.0 0.9 add_convert_fusion
  (30 shorter events, 0.9 us)
Async XLA Ops:
  0.0 11.9 %copy-start.4 = (s32[512]{0:T(512)S(1)}, s32[512]{0:T(512)}, u32[]{:S(2)}) copy-start(s32[512]{0:T(512)} %param.17) | copy-start | bytes 6148
  0.0 12.1 %copy-start.2 = (bf16[512,256]{1,0:T(8,128)(2,1)S(1)}, bf16[512,256]{1,0:T(8,128)(2,1)}, u32[]{:S(2)}) copy-start(bf16[512,256]{1,0:T(8,128)(2,1)} %param.15) | copy-start | bytes 786436
  0.0 23.0 %copy-start.1 = (bf16[128,2048]{1,0:T(8,128)(2,1)S(1)}, bf16[128,2048]{1,0:T(8,128)(2,1)}, u32[]{:S(2)}) copy-start(bf16[128,2048]{1,0:T(8,128)(2,1)} %param.18) | copy-start | bytes 1572868
  1.2 10.9 %collective-permute-start.1 = (f32[2,256]{1,0:T(2,128)S(1)}, f32[2,256]{1,0:T(2,128)S(1)}, u32[]{:S(2)}, u32[]{:S(2)}) collective-permute-start(f32[2,256]{1,0:T(2,128)S(1)} %slice.48), channel_id=1, source_target_pairs={{0,4},{4,8},{8,12},{12,16},{16,20},{20,24},{24,28},{28,32},{32,36}... | collective-permute-start | bytes 6152 | tf_op jit(solution)/shard_map/ppermute | solution.py:10
  6.5 5.4 %collective-permute-start = (s32[2]{0:T(128)S(1)}, s32[2]{0:T(128)S(1)}, u32[]{:S(2)}, u32[]{:S(2)}) collective-permute-start(s32[2]{0:T(128)S(1)} %slice.35), channel_id=1, source_target_pairs={{0,4},{4,8},{8,12},{12,16},{16,20},{20,24},{24,28},{28,32},{32,36}... | collective-permute-start | bytes 32 | tf_op jit(solution)/shard_map/ppermute | solution.py:10
  13.1 9.7 %all-to-all-start = ((bf16[4,128,256]{2,1,0:T(8,128)(2,1)}), bf16[4,128,256]{2,1,0:T(8,128)(2,1)S(1)}, u32[]{:S(2)}, u32[]{:S(2)}) async-start(bf16[4,128,256]{2,1,0:T(8,128)(2,1)} %bitcast.3), calls=%async_computation | async-start | bytes 524288 | tf_op jit(solution)/shard_map/all_to_all | solution.py:48
  23.0 3.0 %copy-start.3 = (f32[2048]{0:T(1024)S(1)}, f32[2048]{0:T(1024)}, u32[]{:S(2)}) copy-start(f32[2048]{0:T(1024)} %param.20) | copy-start | bytes 24580
  76.4 6.7 %copy-start = (bf16[512,2048]{1,0:T(8,128)(2,1)S(1)}, bf16[512,2048]{1,0:T(8,128)(2,1)}, u32[]{:S(2)}) copy-start(bf16[512,2048]{1,0:T(8,128)(2,1)} %reshape.84) | copy-start | bytes 6291460
  97.0 5.0 %copy-start.5 = (f32[128,2]{0,1:T(2,128)S(1)}, f32[128,2]{0,1:T(2,128)}, u32[]{:S(2)}) copy-start(f32[128,2]{0,1:T(2,128)} %param.22) | copy-start | bytes 3076
  97.0 35.5 %all-to-all-start.2 = ((bf16[128,4,2048]{2,1,0:T(4,128)(2,1)}), bf16[128,4,2048]{2,1,0:T(4,128)(2,1)}, u32[]{:S(2)}, u32[]{:S(2)}) async-start(bf16[128,4,2048]{2,1,0:T(4,128)(2,1)} %reshape.85), calls=%async_computation.2 | async-start | bytes 4194304 | tf_op jit(solution)/shard_map/all_to_all | solution.py:84
where the time goes:
time: 145 us; the launch traced here: 144 us
  blocking collectives  40.5 us (28%)
  waiting for transfers between devices  36.1 us (25%)
  local copies, waits for them, and re-layouts  24.3 us (17%)
  matrix products  19.6 us (14%)
  starting transfers between devices  15.5 us (11%)
  other arithmetic  7.76 us (5%)
    all_to_all x1, blocking collectives, on_device(): lax.all_to_all(outgoing.reshape(experts_total, capacity, model_width), ('...  40.5 us
    all_to_all x1, waiting for transfers between devices, on_device(): lax.all_to_all(result, ('sp', 'tp'), split_axis=0, concat_axis=0, tiled=T...  30.4 us
    dot_general x1, matrix products, expert_rows(): jnp.dot(hidden, down_weight, preferred_element_type=jnp.float32)  9.9 us
    dot_general x1, matrix products, expert_rows(): jnp.dot(arrived, gate_weight, preferred_element_type=jnp.float32)  6.65 us
    ppermute x2, starting transfers between devices, from_behind(): return lax.ppermute(block, axis, route)  6.49 us
    all_to_all x1, waiting for transfers between devices, on_device(): lax.all_to_all(conv_out, 'tp', split_axis=0, concat_axis=1, tiled=True)  5.69 us
    all_to_all x1, starting transfers between devices, on_device(): lax.all_to_all(result, ('sp', 'tp'), split_axis=0, concat_axis=0, tiled=T...  4.97 us
    reshape x1, local copies, waits for them, and re-layouts, on_device(): result = result.reshape(experts_total, item_count, model_width)  4.11 us
  transfers between devices with their start and end apart: 4, of which 2 were waited for; matrix products, arithmetic and copies ran while one was open for 3% of the time, Pallas kernels for 0%

commit v1 on v0

--- a/solution.py
+++ b/solution.py
@@ -45,7 +45,10 @@
     mixed_rows = tap_values[2] * inner_prod + tap_values[1] * one_back + tap_values[0] * two_back
     conv_out = (gate_outer.astype(jnp.float32) * mixed_rows).astype(jnp.bfloat16)
     row_count = residual_in.shape[0]
-    regrouped = lax.all_to_all(conv_out, "tp", split_axis=0, concat_axis=1, tiled=True)
+    regrouped = jnp.concatenate(
+        lax.all_to_all(jnp.stack(jnp.split(conv_out, lax.axis_size("tp"), axis=0)), "tp", 0, 0),
+        axis=1,
+    )
     mix = jnp.dot(regrouped, out_proj, preferred_element_type=jnp.float32).astype(jnp.bfloat16)
     carried = residual_in.astype(jnp.float32) + mix.astype(jnp.float32)
     normed = (

time: 145 us -> 143 us (0.986)
  other arithmetic: 7.76 us -> 6.23 us
    unnamed x14 -> x21, local copies, waits for them, and re-layouts: 0.93 us -> 2.62 us
  transfers between devices with their start and end apart: 4 -> 4, of which waited for: 2 -> 2; matrix products, arithmetic and copies ran while one was open for 3% -> 1% of each run, Pallas kernels for 0% -> 0%
where the time goes in v1:
time: 143 us
  blocking collectives  40.5 us (28%)
  waiting for transfers between devices  36.1 us (25%)
  local copies, waits for them, and re-layouts  24.4 us (17%)
  matrix products  19.6 us (14%)
  starting transfers between devices  15.5 us (11%)
  other arithmetic  6.23 us (4%)
    all_to_all x1, blocking collectives, on_device(): lax.all_to_all(outgoing.reshape(experts_total, capacity, model_width), ('...  40.5 us
    all_to_all x1, waiting for transfers between devices, on_device(): lax.all_to_all(result, ('sp', 'tp'), split_axis=0, concat_axis=0, tiled=T...  30.4 us
    dot_general x1, matrix products, expert_rows(): jnp.dot(hidden, down_weight, preferred_element_type=jnp.float32)  9.9 us
    dot_general x1, matrix products, expert_rows(): jnp.dot(arrived, gate_weight, preferred_element_type=jnp.float32)  6.64 us
    ppermute x2, starting transfers between devices, from_behind(): return lax.ppermute(block, axis, route)  6.49 us
    all_to_all x1, waiting for transfers between devices, on_device(): lax.all_to_all(jnp.stack(jnp.split(conv_out, lax.axis_size('tp'), axis=0)...  5.69 us
    all_to_all x1, starting transfers between devices, on_device(): lax.all_to_all(result, ('sp', 'tp'), split_axis=0, concat_axis=0, tiled=T...  4.98 us
    reshape x1, local copies, waits for them, and re-layouts, on_device(): result = result.reshape(experts_total, item_count, model_width)  4.09 us
  transfers between devices with their start and end apart: 4, of which 2 were waited for; matrix products, arithmetic and copies ran while one was open for 1% of the time, Pallas kernels for 0%

profile of v1, /device:TPU:1, one launch (start us, length us, event | category | flops | bytes accessed | tf_op | source)
XLA Modules:
  0.0 142.6 jit_solution(5676852584177588969)
XLA Ops:
  0.0 1.1 copy.16
  1.2 1.1 copy.17
  2.4 4.6 %collective-permute-start.1 = (f32[2,256]{0,1:T(8,128)S(1)}, f32[2,256]{0,1:T(8,128)S(1)}, u32[]{:S(2)}, u32[]{:S(2)}) collective-permute-start(f32[2,256]{0,1:T(8,128)S(1)} %slice.48), channel_id=1, source_target_pairs={{0,4},{4,8},{8,12},{12,16},{16,20},{20,24},{24,28},{28,32},{32,36}... | collective-permute-start | bytes 6152 | tf_op jit(solution)/shard_map/ppermute | solution.py:10
  7.1 1.9 %collective-permute-start = (s32[2]{0:T(128)S(1)}, s32[2]{0:T(128)S(1)}, u32[]{:S(2)}, u32[]{:S(2)}) collective-permute-start(s32[2]{0:T(128)S(1)} %slice.35), channel_id=1, source_target_pairs={{0,4},{4,8},{8,12},{12,16},{16,20},{20,24},{24,28},{28,32},{32,36}... | collective-permute-start | bytes 32 | tf_op jit(solution)/shard_map/ppermute | solution.py:10
  9.2 0.1 eq.37
  9.3 0.1 eq.33
  9.5 0.1 copy.15
  9.8 0.2 fusion.26
  10.2 0.1 mul.103
  10.3 0.2 fusion.27
  10.7 0.5 fusion.23
  11.3 0.7 pad_maximum_fusion.1
  12.0 4.0 %all-to-all-start = ((bf16[4,128,256]{1,2,0:T(8,128)(2,1)}), bf16[4,128,256]{1,2,0:T(8,128)(2,1)S(1)}, u32[]{:S(2)}, u32[]{:S(2)}) async-start(bf16[4,128,256]{1,2,0:T(8,128)(2,1)} %pad_maximum_fusion.1), calls=%async_computation | async-start | bytes 524288 | tf_op jit(solution)/shard_map/all_to_all | solution.py:49
  16.0 5.7 %all-to-all-done = bf16[4,128,256]{1,2,0:T(8,128)(2,1)S(1)} async-done(((bf16[4,128,256]{1,2,0:T(8,128)(2,1)}), bf16[4,128,256]{1,2,0:T(8,128)(2,1)S(1)}, u32[]{:S(2)}, u32[]{:S(2)}) %all-to-all-start) | async-done | bytes 262176 | tf_op jit(solution)/shard_map/all_to_all | solution.py:49
  21.7 3.0 %multiply_reduce_fusion.1 = (f32[128]{0:T(128)S(1)}, f32[128,2048]{1,0:T(8,128)S(1)}) fusion(bf16[128,1024]{0,1:T(8,128)(2,1)S(1)} %bitcast.43, bf16[1024,2048]{1,0:T(8,128)(2,1)} %param.19, bf16[128,2048]{1,0:T(8,128)(2,1)S(1)} %copy-done.1), kind=kOutput, calls=%fused_computation.16 | convolution fusion | flops 538443648 | bytes 6029824 | tf_op jit(solution)/shard_map/dot_general | solution.py:52
  24.8 0.2 multiply_convert_fusion.1
  24.9 0.6 broadcast_in_dim.36
  25.6 1.2 reshape.105
  26.8 3.5 %scatter_custom_fusion = bf16[512,2048]{1,0:T(8,128)(2,1)S(1)} fusion(s32[256]{0:T(256)S(1)} %bitcast.48, bf16[256,2048]{1,0:T(8,128)(2,1)} %reshape.105, bf16[]{:T(256)} %constant.6.clone.1), kind=kCustom, calls=%fused_computation.17 | custom fusion | bytes 2097664 | tf_op jit(solution)/shard_map/scatter | solution.py:71
  30.3 2.2 %reshape.88 = bf16[128,4,2048]{2,1,0:T(4,128)(2,1)} reshape(bf16[512,2048]{1,0:T(8,128)(2,1)S(1)} %scatter_custom_fusion) | data formatting | bytes 4194304 | tf_op jit(solution)/shard_map/reshape | solution.py:77
  32.5 40.5 %all_to_all.15 = bf16[128,4,2048]{2,1,0:T(4,128)(2,1)S(1)} all-to-all(bf16[128,4,2048]{2,1,0:T(4,128)(2,1)} %reshape.88), channel_id=1, replica_groups=mesh['sp'=32,'tp'=4] {'sp','tp'}, dimensions={0} | all-to-all | bytes 4194304 | tf_op jit(solution)/shard_map/all_to_all | solution.py:76
  73.0 2.0 %reshape.89 = bf16[512,2048]{1,0:T(8,128)(2,1)} reshape(bf16[128,4,2048]{2,1,0:T(4,128)(2,1)S(1)} %all_to_all.15) | data formatting | bytes 4194304 | tf_op jit(solution)/shard_map/reshape | solution.py:84
  75.1 6.6 %fusion.4 = f32[512,1024]{1,0:T(8,128)} fusion(bf16[512,2048]{1,0:T(8,128)(2,1)} %reshape.89, bf16[1,2048,1024]{2,1,0:T(8,128)(2,1)} %param.23), kind=kOutput, calls=%fused_computation.6 | convolution fusion | flops 2147483648 | bytes 8388608 | tf_op jit(solution)/shard_map/dot_general | solution.py:14
  81.7 9.9 %fusion.6 = bf16[512,2048]{1,0:T(8,128)(2,1)} fusion(bf16[1,1024,2048]{2,1,0:T(8,128)(2,1)} %param.25, f32[512,1024]{1,0:T(8,128)} %fusion.4, bf16[512,2048]{1,0:T(8,128)(2,1)S(1)} %copy-done, bf16[1,2048,1024]{2,1,0:T(8,128)(2,1)} %param.24), kind=kOutput, calls=%fused_computation.8 | convolution fusion | flops 4299161600 | bytes 14680064 | tf_op jit(solution)/shard_map/dot_general | solution.py:17
  91.6 4.1 %reshape.90 = bf16[128,4,2048]{2,1,0:T(4,128)(2,1)} reshape(bf16[512,2048]{1,0:T(8,128)(2,1)} %fusion.6) | data formatting | bytes 4194304 | tf_op jit(solution)/shard_map/reshape | solution.py:86
  95.7 5.0 %all-to-all-start.2 = ((bf16[128,4,2048]{2,1,0:T(4,128)(2,1)}), bf16[128,4,2048]{2,1,0:T(4,128)(2,1)}, u32[]{:S(2)}, u32[]{:S(2)}) async-start(bf16[128,4,2048]{2,1,0:T(4,128)(2,1)} %reshape.90), calls=%async_computation.2 | async-start | bytes 4194304 | tf_op jit(solution)/shard_map/all_to_all | solution.py:87
  100.8 30.4 %all-to-all-done.2 = bf16[128,4,2048]{2,1,0:T(4,128)(2,1)} async-done(((bf16[128,4,2048]{2,1,0:T(4,128)(2,1)}), bf16[128,4,2048]{2,1,0:T(4,128)(2,1)}, u32[]{:S(2)}, u32[]{:S(2)}) %all-to-all-start.2) | async-done | bytes 2097184 | tf_op jit(solution)/shard_map/all_to_all | solution.py:87
  131.2 2.5 %reshape.91 = bf16[512,2048]{1,0:T(8,128)(2,1)S(1)} reshape(bf16[128,4,2048]{2,1,0:T(4,128)(2,1)} %all-to-all-done.2) | data formatting | bytes 4194304 | tf_op jit(solution)/shard_map/reshape | solution.py:89
  133.8 2.3 %gather_fusion = bf16[256,2048]{1,0:T(8,128)(2,1)} fusion(bf16[512,2048]{1,0:T(8,128)(2,1)S(1)} %reshape.91, s32[1024]{0:T(1024)S(1)} %pad_clamp_fusion), kind=kCustom, calls=%fused_computation | custom fusion | bytes 2098176 | tf_op jit(solution)/shard_map/gather | solution.py:89
  136.1 2.4 %reshape.92 = f32[128,2,2048]{2,1,0:T(2,128)S(1)} reshape(bf16[256,2048]{1,0:T(8,128)(2,1)} %gather_fusion) | data formatting | bytes 3145728 | tf_op jit(solution)/shard_map/convert_element_type | solution.py:91
  138.5 3.2 %multiply_reduce_fusion = f32[128,2048]{1,0:T(8,128)S(1)} fusion(f32[128,2,2048]{2,1,0:T(2,128)S(1)} %reshape.92, f32[128,2]{1,0:T(8,128)S(1)} %copy.18), kind=kLoop, calls=%fused_computation.12 | loop fusion | flops 786432 | bytes 3146752 | tf_op jit(solution)/shard_map/reduce_sum | solution.py:93
  141.7 0.9 add_convert_fusion
  (38 shorter events, 1.1 us)
Async XLA Ops:
  0.0 7.0 %copy-start.4 = (s32[512]{0:T(512)S(1)}, s32[512]{0:T(512)}, u32[]{:S(2)}) copy-start(s32[512]{0:T(512)} %param.17) | copy-start | bytes 6148
  0.0 9.0 %copy-start.6 = (s32[128,2]{0,1:T(2,128)S(1)}, s32[128,2]{0,1:T(2,128)}, u32[]{:S(2)}) copy-start(s32[128,2]{0,1:T(2,128)} %param.21) | copy-start | bytes 3076
  0.0 9.4 %copy-start.5 = (bf16[3,256]{1,0:T(4,128)(2,1)S(1)}, bf16[3,256]{1,0:T(4,128)(2,1)}, u32[]{:S(2)}) copy-start(bf16[3,256]{1,0:T(4,128)(2,1)} %param.16) | copy-start | bytes 4612
  0.0 9.5 %copy-start.2 = (bf16[512,256]{1,0:T(8,128)(2,1)S(1)}, bf16[512,256]{1,0:T(8,128)(2,1)}, u32[]{:S(2)}) copy-start(bf16[512,256]{1,0:T(8,128)(2,1)} %param.15) | copy-start | bytes 786436
  2.4 8.3 %collective-permute-start.1 = (f32[2,256]{0,1:T(8,128)S(1)}, f32[2,256]{0,1:T(8,128)S(1)}, u32[]{:S(2)}, u32[]{:S(2)}) collective-permute-start(f32[2,256]{0,1:T(8,128)S(1)} %slice.48), channel_id=1, source_target_pairs={{0,4},{4,8},{8,12},{12,16},{16,20},{20,24},{24,28},{28,32},{32,36}... | collective-permute-start | bytes 6152 | tf_op jit(solution)/shard_map/ppermute | solution.py:10
  7.1 3.4 %collective-permute-start = (s32[2]{0:T(128)S(1)}, s32[2]{0:T(128)S(1)}, u32[]{:S(2)}, u32[]{:S(2)}) collective-permute-start(s32[2]{0:T(128)S(1)} %slice.35), channel_id=1, source_target_pairs={{0,4},{4,8},{8,12},{12,16},{16,20},{20,24},{24,28},{28,32},{32,36}... | collective-permute-start | bytes 32 | tf_op jit(solution)/shard_map/ppermute | solution.py:10
  9.5 12.2 %copy-start.1 = (bf16[128,2048]{1,0:T(8,128)(2,1)S(1)}, bf16[128,2048]{1,0:T(8,128)(2,1)}, u32[]{:S(2)}) copy-start(bf16[128,2048]{1,0:T(8,128)(2,1)} %param.18) | copy-start | bytes 1572868
  12.0 9.7 %all-to-all-start = ((bf16[4,128,256]{1,2,0:T(8,128)(2,1)}), bf16[4,128,256]{1,2,0:T(8,128)(2,1)S(1)}, u32[]{:S(2)}, u32[]{:S(2)}) async-start(bf16[4,128,256]{1,2,0:T(8,128)(2,1)} %pad_maximum_fusion.1), calls=%async_computation | async-start | bytes 524288 | tf_op jit(solution)/shard_map/all_to_all | solution.py:49
  21.7 3.0 %copy-start.3 = (f32[2048]{0:T(1024)S(1)}, f32[2048]{0:T(1024)}, u32[]{:S(2)}) copy-start(f32[2048]{0:T(1024)} %param.20) | copy-start | bytes 24580
  75.1 6.6 %copy-start = (bf16[512,2048]{1,0:T(8,128)(2,1)S(1)}, bf16[512,2048]{1,0:T(8,128)(2,1)}, u32[]{:S(2)}) copy-start(bf16[512,2048]{1,0:T(8,128)(2,1)} %reshape.89) | copy-start | bytes 6291460
  95.7 5.0 %copy-start.7 = (f32[128,2]{0,1:T(2,128)S(1)}, f32[128,2]{0,1:T(2,128)}, u32[]{:S(2)}) copy-start(f32[128,2]{0,1:T(2,128)} %param.22) | copy-start | bytes 3076
  95.7 35.5 %all-to-all-start.2 = ((bf16[128,4,2048]{2,1,0:T(4,128)(2,1)}), bf16[128,4,2048]{2,1,0:T(4,128)(2,1)}, u32[]{:S(2)}, u32[]{:S(2)}) async-start(bf16[128,4,2048]{2,1,0:T(4,128)(2,1)} %reshape.90), calls=%async_computation.2 | async-start | bytes 4194304 | tf_op jit(solution)/shard_map/all_to_all | solution.py:87
